TPU v7x, 512 devices: a 8x2x16 block of a 8x8x16 slice. The times are simulated.
512 devices in a mesh: grp: 2 (over y), fs: 32 (over z, core), tp: 8 (over x).
Axes of the slice: x: 8, y: 2, z: 16, core: 2. Of those that a mesh axis runs over, the one named last changes fastest.
The devices are a block of a 8x8x16 slice.
Arguments:
- tokens: bfloat16 [24576, 2048], P(('grp', 'fs'), 'tp'), parts along dimension 0, may hold values from -6 to 6
- norm_gain: float32 [2048], P('fs'), may hold values from 0.1 to 1.9
- gate_weight: float32 [32, 2048, 1024], P(None, 'fs', 'tp'), may hold values from -0.125 to 0.125
- up_weight: float32 [32, 2048, 1024], P(None, 'fs', 'tp'), may hold values from -0.125 to 0.125
- down_weight: float32 [32, 1024, 2048], P(None, 'fs', 'tp'), may hold values from -0.1875 to 0.1875
- routes: int32 [24576, 2], P(('grp', 'fs')), parts along dimension 0, may hold values from 0 to 31, as said below
- route_weights: float32 [24576, 2], P(('grp', 'fs')), parts along dimension 0, may hold values from 0.2 to 1
Outputs:
- gate_serve: bfloat16 [64, 2048, 1024], P(('grp', 'fs'), None, 'tp'), parts along dimension 0
- up_serve: bfloat16 [64, 2048, 1024], P(('grp', 'fs'), None, 'tp'), parts along dimension 0
- down_serve: bfloat16 [64, 1024, 2048], P(('grp', 'fs'), None, 'tp'), parts along dimension 0
- mixture: bfloat16 [24576, 2048], P(('grp', 'fs'), 'tp'), parts along dimension 0
There are 2 independent parts, one for each index of `grp`. A program takes and returns all parts, laid end to end along the dimension named above; an argument that names none is the same for every part. Nothing has to cross between parts.
Inputs may be any that keep to these rules, and one draw needn't show every extreme that they name: `routes`: each row names two different experts of one group (expert e lies in group e // 8). In each aligned block of 384 rows no expert is named more than 36 times, and every expert of one group is named exactly 36 times.
All inputs are finite; a program needn't handle non-finite values.
Results may differ from a plain program's by a relative error of at most 0.0087.
Values may be sent and summed in bfloat16 or wider, within the bound.
No kernel may reach another device: no remote copies, remote signals or barrier semaphores. Data moves between devices by JAX's collectives and lax.ppermute only.
A program may use at most 64 MiB of HBM per device.

v0:
```python
import jax
import jax.numpy as jnp
from jax import lax
from jax.sharding import Mesh
from jax.sharding import PartitionSpec as P

CAP = 36
FS = ("fs_0", "fs_1")
GRP_FS = ("grp", "fs_0", "fs_1")
epsilon = 1e-06


def in_blocks(x, dim, length):
    before, after = (x.shape[:dim], x.shape[dim + 1 :])
    return jnp.moveaxis(x.reshape(*before, length, -1, *after), dim, 0)


def laid_out(blocks, dim):
    blocks = jnp.moveaxis(blocks, 0, dim)
    shape = blocks.shape
    return blocks.reshape(*shape[:dim], shape[dim] * shape[dim + 1], *shape[dim + 2 :])


def exchange_in_order(blocks, axes, order):
    shape = [lax.axis_size(a) for a in axes]
    blocks = blocks.reshape(*shape, *blocks.shape[1:])
    for k in order:
        blocks = lax.all_to_all(blocks, axes[k], split_axis=k, concat_axis=k, tiled=True)
    return blocks.reshape(-1, *blocks.shape[len(axes) :])


def exchange_by_chip(x, groups, order, split_dim, concat_dim):
    length = lax.axis_size(groups[0]) * lax.axis_size(groups[1])
    blocks = in_blocks(x, split_dim, length)
    return laid_out(exchange_in_order(blocks, groups, order), concat_dim)


def normalize(rows):
    values = rows.astype(jnp.float32)
    scale = lax.rsqrt(jnp.mean(values * values, axis=-1, keepdims=True) + epsilon)
    return (values * scale).astype(jnp.bfloat16)


def shards(tokens, norm_gain, gate_weight, up_weight, down_weight, routes, route_weights):
    experts = gate_weight.shape[0]
    n_shards = lax.axis_size(FS)
    local_experts = experts // n_shards
    tok_rows = tokens.shape[0]
    gate_low = (norm_gain[None, :, None] * gate_weight).astype(jnp.bfloat16)
    up_low = (norm_gain[None, :, None] * up_weight).astype(jnp.bfloat16)
    down_low = down_weight.astype(jnp.bfloat16)
    gate_serve, up_serve = (
        lax.all_to_all(gate_low, FS, split_axis=0, concat_axis=1, tiled=True),
        lax.all_to_all(up_low, FS, split_axis=0, concat_axis=1, tiled=True),
    )
    flat_routes = routes.reshape(-1)
    expert_ids = lax.iota(jnp.int32, experts)
    onehot = (flat_routes[:, None] == expert_ids[None, :]).astype(jnp.int32)
    position = jnp.sum((jnp.cumsum(onehot, axis=0) - 1) * onehot, axis=1)
    slot_index = (flat_routes * CAP + position).reshape(tok_rows, 2)
    slot_ids = lax.iota(jnp.int32, experts * CAP)
    select = jnp.any(slot_ids[:, None, None] == slot_index[None, :, :], axis=2).astype(jnp.bfloat16)
    outbound = jnp.dot(select, tokens, preferred_element_type=jnp.float32).astype(jnp.bfloat16)
    outbound = outbound.reshape(n_shards, local_experts, CAP, outbound.shape[1])
    arrived = lax.all_to_all(outbound, FS, split_axis=0, concat_axis=2, tiled=True)[0]
    expert_rows = normalize(lax.all_gather(arrived, "tp", axis=2, tiled=True))
    gate_part = jnp.einsum(
        "erd,edh->erh", expert_rows, gate_serve, preferred_element_type=jnp.float32
    )
    up_part = jnp.einsum("erd,edh->erh", expert_rows, up_serve, preferred_element_type=jnp.float32)
    hidden = (jax.nn.silu(gate_part) * up_part).astype(jnp.bfloat16)
    down_serve = lax.all_to_all(down_low, FS, split_axis=0, concat_axis=1, tiled=True)
    expert_out = jnp.einsum(
        "erk,ekd->erd",
        lax.all_gather(hidden, "tp", axis=2, tiled=True),
        down_serve,
        preferred_element_type=jnp.float32,
    ).astype(jnp.bfloat16)
    expert_out = expert_out.reshape(1, local_experts, hidden.shape[1], expert_out.shape[2])
    returned_rows = exchange_by_chip(expert_out, ("fs_0", "fs_1"), (1, 0), 2, 0)
    returned_rows = returned_rows.reshape(experts * CAP, returned_rows.shape[3])
    picked = returned_rows[slot_index]
    mixture = jnp.sum(route_weights[:, :, None] * picked.astype(jnp.float32), axis=1).astype(
        jnp.bfloat16
    )
    return (gate_serve, up_serve, down_serve, mixture)


def solution(mesh):
    split = Mesh(
        mesh.devices.reshape(mesh.shape["grp"], 16, 2, mesh.shape["tp"]),
        ("grp", "fs_0", "fs_1", "tp"),
    )
    placed = (
        P(GRP_FS, "tp"),
        P(FS),
        P(None, FS, "tp"),
        P(None, FS, "tp"),
        P(None, FS, "tp"),
        P(GRP_FS, None),
        P(GRP_FS, None),
    )
    return jax.shard_map(
        shards,
        mesh=split,
        in_specs=placed,
        out_specs=(
            P(GRP_FS, None, "tp"),
            P(GRP_FS, None, "tp"),
            P(GRP_FS, None, "tp"),
            P(GRP_FS, "tp"),
        ),
        check_vma=False,
    )
```

profile of v0, /device:TPU:66, one launch (start us, length us, event | category | flops | bytes accessed | tf_op | source)
XLA Modules:
  0.0 293.5 jit_solution(14518242084303444602)
XLA Ops:
  7.2 0.1 all-gather.4.cloned.1.call-start
  7.3 0.9 copy.41
  8.2 0.1 eq.43
  8.3 0.1 eq.39
  8.5 1.7 reduce-window.6
  10.3 0.3 slice_reduce_fusion
  10.5 0.1 fusion.9
  10.7 0.2 reduce_sum.30
  10.8 0.1 copy.44
  10.9 0.7 compare_select_fusion
  11.6 0.8 fusion.3
  12.4 0.5 convolution_convert_fusion.1
  12.9 0.1 reshape.99
  13.0 82.9 %all_to_all.55 = bf16[32,1,36,256]{3,2,1,0:T(8,128)(2,1)S(1)} all-to-all(bf16[32,1,36,256]{3,2,1,0:T(8,128)(2,1)S(1)} %bitcast.35), channel_id=1, replica_groups=mesh['grp'=2,'fs_0'=16,'fs_1'=2,'tp'=8] {'fs_0','fs_1'}, dimensions={0} | all-to-all | bytes 1179648 | tf_op jit(solution)/shard_map/all_to_all | solution.py:65
  95.9 0.9 squeeze.3
  96.9 0.1 all-gather.4.cloned.1.call-update
  96.9 2.3 multiply_convert_fusion
  99.2 37.1 %all_to_all.56 = bf16[32,64,128]{2,1,0:T(8,128)(2,1)S(1)} all-to-all(bf16[32,64,128]{2,1,0:T(8,128)(2,1)S(1)} %get-tuple-element.7), channel_id=1, replica_groups=mesh['grp'=2,'fs_0'=16,'fs_1'=2,'tp'=8] {'fs_0','fs_1'}, dimensions={0} | all-to-all | bytes 1048576 | tf_op jit(solution)/shard_map/all_to_all | solution.py:53
  136.3 4.8 %all-to-all-start.1 = ((bf16[32,64,128]{2,1,0:T(8,128)(2,1)}), bf16[32,64,128]{2,1,0:T(8,128)(2,1)S(1)}, u32[]{:S(2)}, u32[]{:S(2)}) async-start(bf16[32,64,128]{2,1,0:T(8,128)(2,1)} %get-tuple-element.6), calls=%async_computation.1 | async-start | bytes 1048576 | tf_op jit(solution)/shard_map/all_to_all | solution.py:54
  141.1 0.1 all-gather.6.cloned.1.call-start
  141.2 22.0 %all-gather.4.cloned.1.call-done = bf16[1,1152,2048]{2,1,0:T(8,128)(2,1)} async-done(((bf16[1,1152,256]{2,1,0:T(8,128)(2,1)}), bf16[1,1152,2048]{2,1,0:T(8,128)(2,1)}) %all-gather.4.cloned.1.call-update) | async-done | bytes 4718608 | tf_op jit(solution)/shard_map/all_gather | solution.py:66
  163.2 3.5 %fusion = f32[1152]{0:T(1024)S(1)} fusion(bf16[1,1152,2048]{2,1,0:T(8,128)(2,1)} %all-gather.4.cloned.1.call-done), kind=kLoop, calls=%fused_computation.3 | loop fusion | flops 7076736 | bytes 4723200 | tf_op jit(solution)/shard_map/reduce_sum | solution.py:40
  166.7 0.3 copy-done.1
  167.0 1.5 fusion.6
  168.5 5.8 %all-to-all-done.1 = bf16[32,64,128]{2,1,0:T(8,128)(2,1)S(1)} async-done(((bf16[32,64,128]{2,1,0:T(8,128)(2,1)}), bf16[32,64,128]{2,1,0:T(8,128)(2,1)S(1)}, u32[]{:S(2)}, u32[]{:S(2)}) %all-to-all-start.1) | async-done | bytes 524320 | tf_op jit(solution)/shard_map/all_to_all | solution.py:54
  174.3 4.6 %fusion.4 = bf16[1152,128]{1,0:T(8,128)(2,1)} fusion(bf16[2048,128]{1,0:T(8,128)(2,1)S(1)} %bitcast.38, bf16[1,1152,2048]{2,1,0:T(8,128)(2,1)} %all-gather.4.cloned.1.call-done, f32[1152]{0:T(1024)S(1)} %add_rsqrt_fusion, f32[1152,128]{1,0:T(8,128)S(1)} %fusion.6), kind=kOutput, calls=%fused_computation.11 | convolution fusion | flops 611942400 | bytes 6132224 | tf_op jit(solution)/shard_map/erd,edh->erh/dot_general | solution.py:70
  178.9 0.1 all-gather.6.cloned.1.call-update
  179.0 0.1 convert_element_type.42
  179.0 38.7 %all_to_all.57 = bf16[32,32,256]{2,1,0:T(8,128)(2,1)S(1)} all-to-all(bf16[32,32,256]{2,1,0:T(8,128)(2,1)S(1)} %convert_element_type.42), channel_id=1, replica_groups=mesh['grp'=2,'fs_0'=16,'fs_1'=2,'tp'=8] {'fs_0','fs_1'}, dimensions={0} | all-to-all | bytes 1048576 | tf_op jit(solution)/shard_map/all_to_all | solution.py:72
  217.8 9.2 %all-gather.6.cloned.1.call-done = bf16[1152,1024]{1,0:T(8,128)(2,1)} async-done(((bf16[1152,128]{1,0:T(8,128)(2,1)}), bf16[1152,1024]{1,0:T(8,128)(2,1)}) %all-gather.6.cloned.1.call-update) | async-done | bytes 2359312 | tf_op jit(solution)/shard_map/all_gather | solution.py:75
  226.9 2.4 convolution_convert_fusion
  229.4 0.1 reshape_transpose_reshape_reshape.3
  229.5 0.2 copy.46
  229.7 4.2 %all_to_all.58 = bf16[16,2,1,1,36,256]{5,0,4,3,2,1:T(8,128)(2,1)S(1)} all-to-all(bf16[16,2,1,1,36,256]{5,0,4,3,2,1:T(8,128)(2,1)S(1)} %copy.46), channel_id=1, replica_groups=mesh['grp'=2,'fs_0'=16,'fs_1'=2,'tp'=8] {'fs_1'}, dimensions={1} | all-to-all | bytes 1179648 | tf_op jit(solution)/shard_map/all_to_all | solution.py:28
  233.9 1.4 copy.47
  235.3 13.1 %all-to-all-start.5 = ((bf16[16,2,1,1,36,256]{5,1,4,3,2,0:T(2,128)(2,1)}), bf16[16,2,1,1,36,256]{5,1,4,3,2,0:T(2,128)(2,1)S(1)}, u32[]{:S(2)}, u32[]{:S(2)}) async-start(bf16[16,2,1,1,36,256]{5,1,4,3,2,0:T(2,128)(2,1)} %copy.47), calls=%async_computation.5 | async-start | bytes 1179648 | tf_op jit(solution)/shard_map/all_to_all | solution.py:28
  248.4 0.1 copy.49
  248.6 0.1 reshape.107
  248.7 0.1 copy.40
  248.9 30.4 %all-to-all-done.5 = bf16[16,2,1,1,36,256]{5,1,4,3,2,0:T(2,128)(2,1)S(1)} async-done(((bf16[16,2,1,1,36,256]{5,1,4,3,2,0:T(2,128)(2,1)}), bf16[16,2,1,1,36,256]{5,1,4,3,2,0:T(2,128)(2,1)S(1)}, u32[]{:S(2)}, u32[]{:S(2)}) %all-to-all-start.5) | async-done | bytes 589856 | tf_op jit(solution)/shard_map/all_to_all | solution.py:28
  279.3 0.1 copy.48
  279.3 0.1 reshape_reshape_reshape.3
  279.5 2.7 gather_fusion
  282.1 0.4 reshape.117
  282.5 1.7 multiply_reduce_fusion
  284.2 0.8 copy.55
  285.0 0.8 copy.56
  285.8 0.8 copy.57
  (15 shorter events, 0.1 us)
Async XLA Ops:
  7.2 5.2 %copy-start = (bf16[384,256]{1,0:T(8,128)(2,1)S(1)}, bf16[384,256]{1,0:T(8,128)(2,1)}, u32[]{:S(2)}) copy-start(bf16[384,256]{1,0:T(8,128)(2,1)} %param.7) | copy-start | bytes 589828
  7.2 89.7 %copy-start.3 = (f32[32,64,128]{2,1,0:T(8,128)S(1)}, f32[32,64,128]{2,1,0:T(8,128)}, u32[]{:S(2)}) copy-start(f32[32,64,128]{2,1,0:T(8,128)} %param.10) | copy-start | bytes 3145732
  7.2 89.7 %copy-start.5 = (f32[64]{0:T(128)S(1)}, f32[64]{0:T(128)}, u32[]{:S(2)}) copy-start(f32[64]{0:T(128)} %param.8) | copy-start | bytes 772
  7.2 156.0 %all-gather.4.cloned.1.call-start = ((), (), s32[]{:S(2)}) async-start(), calls=%async_computation.6 | async-start | bytes 5308416 | tf_op jit(solution)/shard_map/all_gather | solution.py:66
  136.3 38.0 %all-to-all-start.1 = ((bf16[32,64,128]{2,1,0:T(8,128)(2,1)}), bf16[32,64,128]{2,1,0:T(8,128)(2,1)S(1)}, u32[]{:S(2)}, u32[]{:S(2)}) async-start(bf16[32,64,128]{2,1,0:T(8,128)(2,1)} %get-tuple-element.6), calls=%async_computation.1 | async-start | bytes 1048576 | tf_op jit(solution)/shard_map/all_to_all | solution.py:54
  141.1 85.8 %all-gather.6.cloned.1.call-start = ((), (), s32[]{:S(2)}) async-start(), calls=%async_computation.7 | async-start | bytes 2654208 | tf_op jit(solution)/shard_map/all_gather | solution.py:75
  163.2 3.8 %copy-start.1 = (bf16[1,1152,2048]{2,1,0:T(8,128)(2,1)S(1)}, bf16[1,1152,2048]{2,1,0:T(8,128)(2,1)}, u32[]{:S(2)}) copy-start(bf16[1,1152,2048]{2,1,0:T(8,128)(2,1)} %all-gather.4.cloned.1.call-done) | copy-start | bytes 14155780
  174.3 4.7 %copy-start.2 = (f32[32,32,256]{2,1,0:T(8,128)S(1)}, f32[32,32,256]{2,1,0:T(8,128)}, u32[]{:S(2)}) copy-start(f32[32,32,256]{2,1,0:T(8,128)} %param.11) | copy-start | bytes 3145732
  229.4 19.4 %copy-start.4 = (f32[384,2]{0,1:T(2,128)S(1)}, f32[384,2]{0,1:T(2,128)}, u32[]{:S(2)}) copy-start(f32[384,2]{0,1:T(2,128)} %param.13) | copy-start | bytes 9220
  235.3 43.9 %all-to-all-start.5 = ((bf16[16,2,1,1,36,256]{5,1,4,3,2,0:T(2,128)(2,1)}), bf16[16,2,1,1,36,256]{5,1,4,3,2,0:T(2,128)(2,1)S(1)}, u32[]{:S(2)}, u32[]{:S(2)}) async-start(bf16[16,2,1,1,36,256]{5,1,4,3,2,0:T(2,128)(2,1)} %copy.47), calls=%async_computation.5 | async-start | bytes 1179648 | tf_op jit(solution)/shard_map/all_to_all | solution.py:28
Sparse Core Ops, SparseCore 0:
  97.0 66.1 all-gather.3
  179.1 47.8 all-gather.5
where the time goes:
time: 294 us; the launch traced here: 293 us
  blocking collectives  163 us (55%)
  waiting for transfers between devices  67.5 us (23%)
  starting transfers between devices  18 us (6%)
  between operations  14.3 us (5%)
  other arithmetic  10.9 us (4%)
  local copies, waits for them, and re-layouts  10.8 us (4%)
  matrix products  8.96 us (3%)
    all_to_all x1, blocking collectives, shards(): lax.all_to_all(outbound, FS, split_axis=0, concat_axis=2, tiled=True)[0]  82.9 us
    all_to_all x1, blocking collectives, shards(): lax.all_to_all(down_low, FS, split_axis=0, concat_axis=1, tiled=True)  38.7 us
    all_to_all x1, blocking collectives, shards(): lax.all_to_all(gate_low, FS, split_axis=0, concat_axis=1, tiled=True)  37.1 us
    all_to_all x1, waiting for transfers between devices, exchange_in_order(): lax.all_to_all(blocks, axes[k], split_axis=k, concat_axis=k, tiled=True)  30.4 us
    all_gather x1, waiting for transfers between devices, shards(): expert_rows = normalize(lax.all_gather(arrived, 'tp', axis=2, tiled=True))  22 us
    all_to_all x1, starting transfers between devices, exchange_in_order(): lax.all_to_all(blocks, axes[k], split_axis=k, concat_axis=k, tiled=True)  13.1 us
    all_gather x1, waiting for transfers between devices, shards(): lax.all_gather(hidden, 'tp', axis=2, tiled=True)  9.16 us
  transfers between devices with their start and end apart: 4, of which 4 were waited for; matrix products, arithmetic and copies ran while one was open for 3% of the time, Pallas kernels for 0%

commit v1 on v0

--- a/solution.py
+++ b/solution.py
@@ -8,6 +8,12 @@
 FS = ("fs_0", "fs_1")
 GRP_FS = ("grp", "fs_0", "fs_1")
 epsilon = 1e-06
+
+
+def trade_parts(array, axis, split, join):
+    shards = jnp.split(array, lax.axis_size(axis), axis=split)
+    got = lax.all_to_all(jnp.stack(shards), axis, 0, 0)
+    return jnp.concatenate(got, axis=join)
 
 
 def in_blocks(x, dim, length):
@@ -50,7 +56,7 @@
     up_low = (norm_gain[None, :, None] * up_weight).astype(jnp.bfloat16)
     down_low = down_weight.astype(jnp.bfloat16)
     gate_serve, up_serve = (
-        lax.all_to_all(gate_low, FS, split_axis=0, concat_axis=1, tiled=True),
+        trade_parts(gate_low, FS, 0, 1),
         lax.all_to_all(up_low, FS, split_axis=0, concat_axis=1, tiled=True),
     )
     flat_routes = routes.reshape(-1)

time: 294 us -> 295 us (level)
  blocking collectives: 163 us -> 82 us
  starting transfers between devices: 18 us -> 62.5 us
  waiting for transfers between devices: 67.5 us -> 104 us
    all_to_all x2 -> x1, blocking collectives: 120 us -> 37.1 us  [trade_parts(): got = lax.all_to_all(jnp.stack(shards), axis, 0, 0)]
    all_to_all x0 -> x1, starting transfers between devices: none -> 44.4 us  [shards(): lax.all_to_all(outbound, FS, split_axis=0, concat_axis=2, tiled=True)[0]]
    all_to_all x0 -> x1, waiting for transfers between devices: none -> 37.4 us  [shards(): lax.all_to_all(outbound, FS, split_axis=0, concat_axis=2, tiled=True)[0]]
  transfers between devices with their start and end apart: 4 -> 5, of which waited for: 4 -> 5; matrix products, arithmetic and copies ran while one was open for 3% -> 2% of each run, Pallas kernels for 0% -> 0%
where the time goes in v1:
time: 295 us; the launch traced here: 294 us
  waiting for transfers between devices  104 us (35%)
  blocking collectives  82 us (28%)
  starting transfers between devices  62.5 us (21%)
  between operations  14.4 us (5%)
  local copies, waits for them, and re-layouts  12 us (4%)
  other arithmetic  9.78 us (3%)
  matrix products  8.98 us (3%)
    all_to_all x1, starting transfers between devices, shards(): lax.all_to_all(outbound, FS, split_axis=0, concat_axis=2, tiled=True)[0]  44.4 us
    all_to_all x1, blocking collectives, shards(): lax.all_to_all(down_low, FS, split_axis=0, concat_axis=1, tiled=True)  40.7 us
    all_to_all x1, waiting for transfers between devices, shards(): lax.all_to_all(outbound, FS, split_axis=0, concat_axis=2, tiled=True)[0]  37.4 us
    all_to_all x1, blocking collectives, trade_parts(): got = lax.all_to_all(jnp.stack(shards), axis, 0, 0)  37.1 us
    all_to_all x1, waiting for transfers between devices, exchange_in_order(): lax.all_to_all(blocks, axes[k], split_axis=k, concat_axis=k, tiled=True)  30.4 us
    all_gather x1, waiting for transfers between devices, shards(): expert_rows = normalize(lax.all_gather(arrived, 'tp', axis=2, tiled=True))  23.6 us
    all_to_all x1, starting transfers between devices, exchange_in_order(): lax.all_to_all(blocks, axes[k], split_axis=k, concat_axis=k, tiled=True)  13.1 us
    all_gather x1, waiting for transfers between devices, shards(): lax.all_gather(hidden, 'tp', axis=2, tiled=True)  8.71 us
  transfers between devices with their start and end apart: 5, of which 5 were waited for; matrix products, arithmetic and copies ran while one was open for 2% of the time, Pallas kernels for 0%

profile of v1, /device:TPU:66, one launch (start us, length us, event | category | flops | bytes accessed | tf_op | source)
XLA Modules:
  0.0 294.1 jit_solution(4648277082027423270)
XLA Ops:
  7.2 1.0 copy.41
  8.2 0.1 eq.43
  8.4 0.1 eq.39
  8.5 1.7 reduce-window.6
  10.3 0.3 slice_reduce_fusion
  10.5 0.1 fusion.9
  10.7 0.2 reduce_sum.30
  10.8 0.1 copy.44
  10.9 0.7 compare_select_fusion
  11.6 0.8 fusion.3
  12.4 0.5 convolution_convert_fusion.1
  12.9 1.0 reshape.100
  13.8 44.4 %all-to-all-start.3 = ((bf16[32,1,36,256]{3,2,1,0:T(8,128)(2,1)}), bf16[32,1,36,256]{3,2,1,0:T(8,128)(2,1)S(1)}, u32[]{:S(2)}, u32[]{:S(2)}) async-start(bf16[32,1,36,256]{3,2,1,0:T(8,128)(2,1)} %bitcast.36), calls=%async_computation.3 | async-start | bytes 1310720 | tf_op jit(solution)/shard_map/all_to_all | solution.py:71
  58.3 0.1 all-gather.4.cloned.1.call-start
  58.4 1.1 multiply_convert_fusion
  59.6 37.4 %all-to-all-done.3 = bf16[32,1,36,256]{3,2,1,0:T(8,128)(2,1)S(1)} async-done(((bf16[32,1,36,256]{3,2,1,0:T(8,128)(2,1)}), bf16[32,1,36,256]{3,2,1,0:T(8,128)(2,1)S(1)}, u32[]{:S(2)}, u32[]{:S(2)}) %all-to-all-start.3) | async-done | bytes 589856 | tf_op jit(solution)/shard_map/all_to_all | solution.py:71
  97.0 0.9 squeeze.3
  97.9 0.1 all-gather.4.cloned.1.call-update
  98.3 37.1 %all_to_all.48 = bf16[32,1,64,128]{3,2,1,0:T(8,128)(2,1)S(1)} all-to-all(bf16[32,1,64,128]{3,2,1,0:T(8,128)(2,1)S(1)} %constant_dynamic-update-slice_fusion), channel_id=1, replica_groups=mesh['grp'=2,'fs_0'=16,'fs_1'=2,'tp'=8] {'fs_0','fs_1'}, dimensions={0} | all-to-all | bytes 1048576 | tf_op jit(solution)/shard_map/all_to_all | solution.py:15
  135.4 4.8 %all-to-all-start.1 = ((bf16[32,64,128]{2,1,0:T(8,128)(2,1)}), bf16[32,64,128]{2,1,0:T(8,128)(2,1)S(1)}, u32[]{:S(2)}, u32[]{:S(2)}) async-start(bf16[32,64,128]{2,1,0:T(8,128)(2,1)} %get-tuple-element.6), calls=%async_computation.1 | async-start | bytes 1048576 | tf_op jit(solution)/shard_map/all_to_all | solution.py:60
  140.2 0.1 all-gather.6.cloned.1.call-start
  140.2 23.6 %all-gather.4.cloned.1.call-done = bf16[1,1152,2048]{2,1,0:T(8,128)(2,1)} async-done(((bf16[1,1152,256]{2,1,0:T(8,128)(2,1)}), bf16[1,1152,2048]{2,1,0:T(8,128)(2,1)}) %all-gather.4.cloned.1.call-update) | async-done | bytes 4718608 | tf_op jit(solution)/shard_map/all_gather | solution.py:72
  163.8 3.5 %fusion = f32[1152]{0:T(1024)S(1)} fusion(bf16[1,1152,2048]{2,1,0:T(8,128)(2,1)} %all-gather.4.cloned.1.call-done), kind=kLoop, calls=%fused_computation.3 | loop fusion | flops 7076736 | bytes 4723200 | tf_op jit(solution)/shard_map/reduce_sum | solution.py:46
  167.3 0.3 copy-done.1
  167.6 1.5 fusion.6
  169.1 4.3 %all-to-all-done.1 = bf16[32,64,128]{2,1,0:T(8,128)(2,1)S(1)} async-done(((bf16[32,64,128]{2,1,0:T(8,128)(2,1)}), bf16[32,64,128]{2,1,0:T(8,128)(2,1)S(1)}, u32[]{:S(2)}, u32[]{:S(2)}) %all-to-all-start.1) | async-done | bytes 524320 | tf_op jit(solution)/shard_map/all_to_all | solution.py:60
  173.3 4.6 %fusion.4 = bf16[1152,128]{1,0:T(8,128)(2,1)} fusion(bf16[2048,128]{1,0:T(8,128)(2,1)S(1)} %bitcast.165, bf16[1,1152,2048]{2,1,0:T(8,128)(2,1)} %all-gather.4.cloned.1.call-done, f32[1152]{0:T(1024)S(1)} %add_rsqrt_fusion, f32[1152,128]{1,0:T(8,128)S(1)} %fusion.6), kind=kOutput, calls=%fused_computation.11 | convolution fusion | flops 611942400 | bytes 6132224 | tf_op jit(solution)/shard_map/erd,edh->erh/dot_general | solution.py:76
  178.0 0.1 convert_element_type.42
  178.1 40.7 %all_to_all.49 = bf16[32,32,256]{2,1,0:T(8,128)(2,1)S(1)} all-to-all(bf16[32,32,256]{2,1,0:T(8,128)(2,1)S(1)} %convert_element_type.42), channel_id=1, replica_groups=mesh['grp'=2,'fs_0'=16,'fs_1'=2,'tp'=8] {'fs_0','fs_1'}, dimensions={0} | all-to-all | bytes 1048576 | tf_op jit(solution)/shard_map/all_to_all | solution.py:78
  218.8 8.7 %all-gather.6.cloned.1.call-done = bf16[1152,1024]{1,0:T(8,128)(2,1)} async-done(((bf16[1152,128]{1,0:T(8,128)(2,1)}), bf16[1152,1024]{1,0:T(8,128)(2,1)}) %all-gather.6.cloned.1.call-update) | async-done | bytes 2359312 | tf_op jit(solution)/shard_map/all_gather | solution.py:81
  227.5 2.4 convolution_convert_fusion
  230.0 0.1 reshape_transpose_reshape_reshape.3
  230.1 0.2 copy.46
  230.3 4.2 %all_to_all.50 = bf16[16,2,1,1,36,256]{5,0,4,3,2,1:T(8,128)(2,1)S(1)} all-to-all(bf16[16,2,1,1,36,256]{5,0,4,3,2,1:T(8,128)(2,1)S(1)} %copy.46), channel_id=1, replica_groups=mesh['grp'=2,'fs_0'=16,'fs_1'=2,'tp'=8] {'fs_1'}, dimensions={1} | all-to-all | bytes 1179648 | tf_op jit(solution)/shard_map/all_to_all | solution.py:34
  234.5 1.4 copy.47
  236.0 13.1 %all-to-all-start.5 = ((bf16[16,2,1,1,36,256]{5,1,4,3,2,0:T(2,128)(2,1)}), bf16[16,2,1,1,36,256]{5,1,4,3,2,0:T(2,128)(2,1)S(1)}, u32[]{:S(2)}, u32[]{:S(2)}) async-start(bf16[16,2,1,1,36,256]{5,1,4,3,2,0:T(2,128)(2,1)} %copy.47), calls=%async_computation.5 | async-start | bytes 1179648 | tf_op jit(solution)/shard_map/all_to_all | solution.py:34
  249.1 0.1 copy.49
  249.2 0.1 reshape.108
  249.4 0.1 copy.40
  249.5 30.4 %all-to-all-done.5 = bf16[16,2,1,1,36,256]{5,1,4,3,2,0:T(2,128)(2,1)S(1)} async-done(((bf16[16,2,1,1,36,256]{5,1,4,3,2,0:T(2,128)(2,1)}), bf16[16,2,1,1,36,256]{5,1,4,3,2,0:T(2,128)(2,1)S(1)}, u32[]{:S(2)}, u32[]{:S(2)}) %all-to-all-start.5) | async-done | bytes 589856 | tf_op jit(solution)/shard_map/all_to_all | solution.py:34
  279.9 0.1 copy.48
  280.0 0.1 reshape_reshape_reshape.3
  280.1 2.7 gather_fusion
  282.8 0.4 reshape.118
  283.1 1.7 multiply_reduce_fusion
  284.9 0.8 copy.86
  285.7 0.8 copy.87
  286.5 0.8 copy.88
  (50 shorter events, 0.4 us)
Async XLA Ops:
  7.2 5.2 %copy-start = (bf16[384,256]{1,0:T(8,128)(2,1)S(1)}, bf16[384,256]{1,0:T(8,128)(2,1)}, u32[]{:S(2)}) copy-start(bf16[384,256]{1,0:T(8,128)(2,1)} %param.7) | copy-start | bytes 589828
  7.2 51.2 %copy-start.3 = (f32[32,64,128]{2,1,0:T(8,128)S(1)}, f32[32,64,128]{2,1,0:T(8,128)}, u32[]{:S(2)}) copy-start(f32[32,64,128]{2,1,0:T(8,128)} %param.10) | copy-start | bytes 3145732
  7.2 51.2 %copy-start.6 = (f32[64]{0:T(128)S(1)}, f32[64]{0:T(128)}, u32[]{:S(2)}) copy-start(f32[64]{0:T(128)} %param.8) | copy-start | bytes 772
  7.2 51.2 %copy-start.4 = (f32[32,64,128]{2,1,0:T(8,128)S(1)}, f32[32,64,128]{2,1,0:T(8,128)}, u32[]{:S(2)}) copy-start(f32[32,64,128]{2,1,0:T(8,128)} %param.9) | copy-start | bytes 3145732
  13.8 83.1 %all-to-all-start.3 = ((bf16[32,1,36,256]{3,2,1,0:T(8,128)(2,1)}), bf16[32,1,36,256]{3,2,1,0:T(8,128)(2,1)S(1)}, u32[]{:S(2)}, u32[]{:S(2)}) async-start(bf16[32,1,36,256]{3,2,1,0:T(8,128)(2,1)} %bitcast.36), calls=%async_computation.3 | async-start | bytes 1310720 | tf_op jit(solution)/shard_map/all_to_all | solution.py:71
  58.3 105.6 %all-gather.4.cloned.1.call-start = ((), (), s32[]{:S(2)}) async-start(), calls=%async_computation.6 | async-start | bytes 5308416 | tf_op jit(solution)/shard_map/all_gather | solution.py:72
  135.4 38.0 %all-to-all-start.1 = ((bf16[32,64,128]{2,1,0:T(8,128)(2,1)}), bf16[32,64,128]{2,1,0:T(8,128)(2,1)S(1)}, u32[]{:S(2)}, u32[]{:S(2)}) async-start(bf16[32,64,128]{2,1,0:T(8,128)(2,1)} %get-tuple-element.6), calls=%async_computation.1 | async-start | bytes 1048576 | tf_op jit(solution)/shard_map/all_to_all | solution.py:60
  140.2 87.4 %all-gather.6.cloned.1.call-start = ((), (), s32[]{:S(2)}) async-start(), calls=%async_computation.7 | async-start | bytes 2654208 | tf_op jit(solution)/shard_map/all_gather | solution.py:81
  163.8 3.8 %copy-start.1 = (bf16[1,1152,2048]{2,1,0:T(8,128)(2,1)S(1)}, bf16[1,1152,2048]{2,1,0:T(8,128)(2,1)}, u32[]{:S(2)}) copy-start(bf16[1,1152,2048]{2,1,0:T(8,128)(2,1)} %all-gather.4.cloned.1.call-done) | copy-start | bytes 14155780
  173.3 4.7 %copy-start.2 = (f32[32,32,256]{2,1,0:T(8,128)S(1)}, f32[32,32,256]{2,1,0:T(8,128)}, u32[]{:S(2)}) copy-start(f32[32,32,256]{2,1,0:T(8,128)} %param.11) | copy-start | bytes 3145732
  230.0 19.4 %copy-start.5 = (f32[384,2]{0,1:T(2,128)S(1)}, f32[384,2]{0,1:T(2,128)}, u32[]{:S(2)}) copy-start(f32[384,2]{0,1:T(2,128)} %param.13) | copy-start | bytes 9220
  236.0 43.9 %all-to-all-start.5 = ((bf16[16,2,1,1,36,256]{5,1,4,3,2,0:T(2,128)(2,1)}), bf16[16,2,1,1,36,256]{5,1,4,3,2,0:T(2,128)(2,1)S(1)}, u32[]{:S(2)}, u32[]{:S(2)}) async-start(bf16[16,2,1,1,36,256]{5,1,4,3,2,0:T(2,128)(2,1)} %copy.47), calls=%async_computation.5 | async-start | bytes 1179648 | tf_op jit(solution)/shard_map/all_to_all | solution.py:34
Sparse Core Ops, SparseCore 0:
  98.1 65.7 all-gather.3
  178.1 49.3 all-gather.5
